TPU v7x, 256 devices: a 4x2x16 block of a 4x16x16 slice. The times are simulated.
256 devices in a mesh: grp: 2 (over y), ep: 32 (over z, core), tp: 4 (over x).
Axes of the slice: x: 4, y: 2, z: 16, core: 2. Of those that a mesh axis runs over, the one named last changes fastest.
The devices are a block of a 4x16x16 slice.
Arguments:
- tokens: bfloat16 [32768, 2048], P(('grp', 'ep', 'tp')), parts along dimension 0, may hold values from -6 to 6
- norm_gain: float32 [2048], replicated, may hold values from 0.1 to 1.9
- route_ids: int32 [32768, 2], P(('grp', 'ep', 'tp')), parts along dimension 0, may hold values from 0 to 127, all different within a row; in each aligned block of 128 rows (0 to 127, 128 to 255, ...) at most 3 rows name the same one
- route_weights: float32 [32768, 2], P(('grp', 'ep', 'tp')), parts along dimension 0, may hold values from 0.1 to 0.9
- w_gate: bfloat16 [128, 2048, 512], P(('ep', 'tp')), may hold values from -0.125 to 0.125
- w_up: bfloat16 [128, 2048, 512], P(('ep', 'tp')), may hold values from -0.125 to 0.125
- w_down: bfloat16 [128, 512, 2048], P(('ep', 'tp')), may hold values from -0.25 to 0.25
Outputs:
- mixed: bfloat16 [32768, 2048], P(('grp', 'ep', 'tp')), parts along dimension 0
There are 2 independent parts, one for each index of `grp`. A program takes and returns all parts, laid end to end along the dimension named above; an argument that names none is the same for every part. Nothing has to cross between parts.
Inputs may be any that keep to these rules, and one draw needn't show every extreme that they name: `route_ids`: each token names 2 different experts. Among the tokens of one device (aligned blocks of 128 tokens) no expert is named more than 3 times, a bound that some block reaches.
All inputs are finite; a program needn't handle non-finite values.
Results may differ from a plain program's by a relative error of at most 0.0071.
Values may be sent and summed in bfloat16 or wider, within the bound.
No kernel may reach another device: no remote copies, remote signals or barrier semaphores. Data moves between devices by JAX's collectives and lax.ppermute only.
A program may use at most 64 MiB of HBM per device.

v0:
```python
import jax
import jax.numpy as jnp
from jax import lax
from jax.sharding import PartitionSpec as P


def on_device(tokens, norm_gain, route_ids, route_weights, w_gate, w_up, w_down):
    tok_rows, model_width = tokens.shape
    top_count = route_ids.shape[1]
    ep_count = lax.axis_size("ep")
    tp_count = lax.axis_size("tp")
    experts = ep_count * tp_count
    capacity = 3 * tok_rows * top_count // (2 * experts)
    values = tokens.astype(jnp.float32)
    normed = (
        values * lax.rsqrt(jnp.mean(values * values, axis=-1, keepdims=True) + 1e-06) * norm_gain
    ).astype(jnp.bfloat16)
    flat_ids = route_ids.reshape(-1)
    onehot = (flat_ids[:, None] == jnp.arange(experts, dtype=jnp.int32)[None, :]).astype(jnp.int32)
    slot_index = jnp.sum((jnp.cumsum(onehot, axis=0) - onehot) * onehot, axis=-1)
    token_of = jnp.arange(tok_rows * top_count, dtype=jnp.int32) // top_count
    buffer = jnp.zeros((experts, capacity, model_width), jnp.bfloat16)
    buffer = buffer.at[flat_ids, slot_index].set(normed[token_of])
    received = lax.all_to_all(buffer, ("ep", "tp"), split_axis=0, concat_axis=0, tiled=True)
    flat_rows = received.reshape(-1, model_width)
    gate_act = jnp.dot(flat_rows, w_gate[0], preferred_element_type=jnp.float32)
    up_act = jnp.dot(flat_rows, w_up[0], preferred_element_type=jnp.float32)
    hidden = (jax.nn.silu(gate_act) * up_act).astype(jnp.bfloat16)
    result = jnp.dot(hidden, w_down[0], preferred_element_type=jnp.float32).astype(jnp.bfloat16)
    returned = lax.all_to_all(
        result.reshape(received.shape), ("ep", "tp"), split_axis=0, concat_axis=0, tiled=True
    )
    picked = (
        returned[flat_ids, slot_index].reshape(tok_rows, top_count, model_width).astype(jnp.float32)
    )
    return jnp.sum(picked * route_weights[:, :, None], axis=1).astype(jnp.bfloat16)


def solution(mesh):
    return jax.shard_map(
        on_device,
        mesh=mesh,
        in_specs=(
            P(("grp", "ep", "tp"), None),
            P(),
            P(("grp", "ep", "tp"), None),
            P(("grp", "ep", "tp"), None),
            P(("ep", "tp"), None, None),
            P(("ep", "tp"), None, None),
            P(("ep", "tp"), None, None),
        ),
        out_specs=P(("grp", "ep", "tp"), None),
        check_vma=False,
    )
```

profile of v0, /device:TPU:33, one launch (start us, length us, event | category | flops | bytes accessed | tf_op | source)
XLA Modules:
  0.0 326.5 jit_solution(7050438241632619832)
XLA Ops:
  0.0 0.9 copy.18
  0.9 0.1 eq.29
  1.1 0.1 eq.25
  1.2 0.1 reshape.123
  1.5 0.2 fusion.22
  1.8 1.2 fusion.11
  3.1 0.2 fusion.24
  3.3 0.9 fusion.13
  4.2 2.3 gather_fusion
  6.5 1.3 broadcast_in_dim.2
  7.8 0.1 copy-done.1
  8.0 44.7 %scatter_fusion = bf16[128,3,2048]{2,0,1:T(8,128)(2,1)} fusion(bf16[128,3,2048]{2,0,1:T(8,128)(2,1)} %broadcast_in_dim.2, s32[256]{0:T(256)S(1)} %bitcast.35, bf16[256,2048]{1,0:T(8,128)(2,1)S(1)} %copy-done.1), kind=kCustom, calls=%fused_computation.2 | custom fusion | bytes 3147776 | tf_op jit(solution)/shard_map/scatter | solution.py:23
  52.7 2.8 copy.23
  55.4 128.7 %all_to_all.10 = bf16[128,3,2048]{2,1,0:T(4,128)(2,1)} all-to-all(bf16[128,3,2048]{2,1,0:T(4,128)(2,1)S(1)} %copy.23), channel_id=1, replica_groups=mesh['grp'=2,'ep'=32,'tp'=4] {'ep','tp'}, dimensions={0} | all-to-all | bytes 3145728 | tf_op jit(solution)/shard_map/all_to_all | solution.py:24
  184.2 5.1 %reshape.125 = bf16[384,2048]{1,0:T(8,128)(2,1)} reshape(bf16[128,3,2048]{2,1,0:T(4,128)(2,1)} %all_to_all.10) | data formatting | bytes 3145728 | tf_op jit(solution)/shard_map/reshape | solution.py:25
  189.2 3.0 fusion.3
  192.3 5.1 %convolution_convert_fusion = bf16[384,2048]{1,0:T(8,128)(2,1)} fusion(bf16[1,512,2048]{2,1,0:T(8,128)(2,1)S(1)} %copy-done, bf16[384,2048]{1,0:T(8,128)(2,1)} %reshape.125, bf16[1,2048,512]{2,1,0:T(8,128)(2,1)} %param.12, f32[384,512]{1,0:T(8,128)S(1)} %fusion.3), kind=kOutput, calls=%fused_computation.3 | convolution fusion | flops 1612578816 | bytes 8126464 | tf_op jit(solution)/shard_map/dot_general | solution.py:29
  197.4 5.2 %reshape.126 = bf16[128,3,2048]{2,1,0:T(4,128)(2,1)} reshape(bf16[384,2048]{1,0:T(8,128)(2,1)} %convolution_convert_fusion) | data formatting | bytes 3145728 | tf_op jit(solution)/shard_map/reshape | solution.py:31
  202.6 10.0 %all-to-all-start.1 = ((bf16[128,3,2048]{2,1,0:T(4,128)(2,1)}), bf16[128,3,2048]{2,1,0:T(4,128)(2,1)}, u32[]{:S(2)}, u32[]{:S(2)}) async-start(bf16[128,3,2048]{2,1,0:T(4,128)(2,1)} %reshape.126), calls=%async_computation.1 | async-start | bytes 4194304 | tf_op jit(solution)/shard_map/all_to_all | solution.py:30
  212.7 97.8 %all-to-all-done.1 = bf16[128,3,2048]{2,1,0:T(4,128)(2,1)} async-done(((bf16[128,3,2048]{2,1,0:T(4,128)(2,1)}), bf16[128,3,2048]{2,1,0:T(4,128)(2,1)}, u32[]{:S(2)}, u32[]{:S(2)}) %all-to-all-start.1) | async-done | bytes 1572896 | tf_op jit(solution)/shard_map/all_to_all | solution.py:30
  310.5 3.9 %copy.24 = bf16[128,3,2048]{2,0,1:T(8,128)(2,1)} copy(bf16[128,3,2048]{2,1,0:T(4,128)(2,1)} %all-to-all-done.1) | data formatting | bytes 3145728 | tf_op jit(solution)/shard_map/all_to_all | solution.py:30
  314.4 4.1 %gather_fusion.1 = bf16[256,2048]{1,0:T(8,128)(2,1)S(1)} fusion(bf16[128,3,2048]{2,0,1:T(8,128)(2,1)} %copy.24, s32[256]{0:T(256)S(1)} %bitcast.34), kind=kCustom, calls=%fused_computation.1 | custom fusion | bytes 2099200 | tf_op jit(solution)/shard_map/gather | solution.py:34
  318.6 2.4 reshape.127
  320.9 5.6 %multiply_reduce_fusion = bf16[128,2048]{1,0:T(8,128)(2,1)} fusion(f32[128,2,2048]{2,1,0:T(2,128)} %reshape.127, f32[128,2]{1,0:T(8,128)S(1)} %copy.25), kind=kLoop, calls=%fused_computation.9 | loop fusion | flops 786432 | bytes 2622464 | tf_op jit(solution)/shard_map/reduce_sum | solution.py:36
  (19 shorter events, 0.4 us)
Async XLA Ops:
  0.0 192.3 %copy-start = (bf16[1,512,2048]{2,1,0:T(8,128)(2,1)S(1)}, bf16[1,512,2048]{2,1,0:T(8,128)(2,1)}, u32[]{:S(2)}) copy-start(bf16[1,512,2048]{2,1,0:T(8,128)(2,1)} %param.13) | copy-start | bytes 6291460
  0.0 3.3 copy-start.2
  6.5 1.5 copy-start.1
  202.6 10.0 %copy-start.3 = (f32[128,2]{0,1:T(2,128)S(1)}, f32[128,2]{0,1:T(2,128)}, u32[]{:S(2)}) copy-start(f32[128,2]{0,1:T(2,128)} %param.10) | copy-start | bytes 3076
  202.6 107.9 %all-to-all-start.1 = ((bf16[128,3,2048]{2,1,0:T(4,128)(2,1)}), bf16[128,3,2048]{2,1,0:T(4,128)(2,1)}, u32[]{:S(2)}, u32[]{:S(2)}) async-start(bf16[128,3,2048]{2,1,0:T(4,128)(2,1)} %reshape.126), calls=%async_computation.1 | async-start | bytes 4194304 | tf_op jit(solution)/shard_map/all_to_all | solution.py:30
where the time goes:
time: 329 us; the launch traced here: 327 us
  blocking collectives  129 us (39%)
  waiting for transfers between devices  97.8 us (30%)
  local copies, waits for them, and re-layouts  73.5 us (22%)
  starting transfers between devices  10 us (3%)
  matrix products  8.19 us (2%)
  other arithmetic  8.17 us (2%)
    all_to_all x1, blocking collectives, on_device(): lax.all_to_all(buffer, ('ep', 'tp'), split_axis=0, concat_axis=0, tiled=T...  129 us
    all_to_all x1, waiting for transfers between devices, on_device(): lax.all_to_all(result.reshape(received.shape), ('ep', 'tp'), split_axis=0...  97.8 us
    scatter x2, local copies, waits for them, and re-layouts, on_device(): buffer = buffer.at[flat_ids, slot_index].set(normed[token_of])  47.5 us
    all_to_all x1, starting transfers between devices, on_device(): lax.all_to_all(result.reshape(received.shape), ('ep', 'tp'), split_axis=0...  10 us
  transfers between devices with their start and end apart: 1, of which 1 were waited for; matrix products, arithmetic and copies ran while one was open for 0% of the time, Pallas kernels for 0%

commit v1 on v0

v1 whole, which is shorter than its diff:
```python
import jax
import jax.numpy as jnp
from jax import lax
from jax.sharding import PartitionSpec as P

LANES = 128


def on_device(tokens, norm_gain, route_ids, route_weights, w_gate, w_up, w_down):
    tok_rows, model_width = tokens.shape
    top_count = route_ids.shape[1]
    experts = lax.axis_size("ep") * lax.axis_size("tp")
    capacity = 3 * tok_rows * top_count // (2 * experts)
    values = tokens.astype(jnp.float32)
    normed = (
        values * lax.rsqrt(jnp.mean(values * values, axis=-1, keepdims=True) + 1e-06) * norm_gain
    ).astype(jnp.bfloat16)
    experts_iota = jnp.arange(experts, dtype=jnp.int32)[:, None]
    ids = route_ids.T
    picks = [ids[k][None, :] == experts_iota for k in range(top_count)]
    named = picks[0]
    for pick in picks[1:]:
        named = named | pick
    earlier = jnp.triu(jnp.ones((tok_rows, tok_rows), jnp.bfloat16), 1)
    rank = jnp.dot(named.astype(jnp.bfloat16), earlier, preferred_element_type=jnp.float32)
    slots = jnp.arange(capacity, dtype=jnp.float32)[None, :, None]
    in_slot = rank[:, None, :] == slots

    def table(mask):
        chosen = (mask[:, None, :] & in_slot).astype(jnp.bfloat16)
        return chosen.reshape(experts * capacity, tok_rows)

    sent = jnp.dot(table(named), normed, preferred_element_type=jnp.float32).astype(jnp.bfloat16)

    def exchange(rows):
        blocks = rows.reshape(experts, capacity * model_width // LANES, LANES)
        moved = lax.all_to_all(blocks, ("ep", "tp"), split_axis=0, concat_axis=0, tiled=True)
        return moved.reshape(experts * capacity, model_width)

    flat_rows = exchange(sent)
    gate_act = jnp.dot(flat_rows, w_gate[0], preferred_element_type=jnp.float32)
    up_act = jnp.dot(flat_rows, w_up[0], preferred_element_type=jnp.float32)
    hidden = (jax.nn.silu(gate_act) * up_act).astype(jnp.bfloat16)
    result = jnp.dot(hidden, w_down[0], preferred_element_type=jnp.float32).astype(jnp.bfloat16)
    returned = exchange(result)
    mixed = jnp.zeros((tok_rows, model_width), jnp.float32)
    for k in range(top_count):
        picked = lax.dot_general(
            table(picks[k]), returned, (((0,), (0,)), ((), ())), preferred_element_type=jnp.float32
        )
        mixed = mixed + picked * route_weights[:, k : k + 1]
    return mixed.astype(jnp.bfloat16)


def solution(mesh):
    return jax.shard_map(
        on_device,
        mesh=mesh,
        in_specs=(
            P(("grp", "ep", "tp"), None),
            P(),
            P(("grp", "ep", "tp"), None),
            P(("grp", "ep", "tp"), None),
            P(("ep", "tp"), None, None),
            P(("ep", "tp"), None, None),
            P(("ep", "tp"), None, None),
        ),
        out_specs=P(("grp", "ep", "tp"), None),
        check_vma=False,
    )
```

time: 329 us -> 223 us (0.68)
  local copies, waits for them, and re-layouts: 73.5 us -> 16.5 us
  waiting for transfers between devices: 97.8 us -> 75.6 us
  blocking collectives: 129 us -> 107 us
  other arithmetic: 8.17 us -> 0.42 us
  matrix products: 8.19 us -> 13.4 us
    scatter x2 -> x0, local copies, waits for them, and re-layouts: 47.5 us -> none  [on_device(): buffer = buffer.at[flat_ids, slot_index].set(normed[token_of])]
    all_to_all x1, waiting for transfers between devices: 97.8 us -> 75.6 us  [exchange(): lax.all_to_all(blocks, ('ep', 'tp'), split_axis=0, concat_axis=0, tiled=T...]
    all_to_all x1, blocking collectives: 129 us -> 107 us  [exchange(): lax.all_to_all(blocks, ('ep', 'tp'), split_axis=0, concat_axis=0, tiled=T...]
    gather x2 -> x0, local copies, waits for them, and re-layouts: 6.47 us -> none  [the longest x1 4.15 us: on_device(): returned[flat_ids, slot_index].reshape(tok_rows, top_count, model_width)]
    reduce_sum x2 -> x0, other arithmetic: 5.77 us -> none  [the longest x1 5.59 us: on_device(): jnp.sum(picked * route_weights[:, :, None], axis=1).astype(jnp.bfloat16)]
    dot_general x0 -> x4, matrix products: none -> 5.24 us  [the longest x2 3.29 us: on_device(): lax.dot_general(table(picks[k]), returned, (((0,), (0,)), ((), ())), pref...]
    reshape x3 -> x4, local copies, waits for them, and re-layouts: 10.4 us -> 14.9 us  [the longest x2 7.52 us: exchange(): blocks = rows.reshape(experts, capacity * model_width // LANES, LANES)]
    all_to_all x1 -> x0, local copies, waits for them, and re-layouts: 3.88 us -> none  [on_device(): lax.all_to_all(result.reshape(received.shape), ('ep', 'tp'), split_axis=0...]
where the time goes in v1:
time: 223 us
  blocking collectives  107 us (48%)
  waiting for transfers between devices  75.6 us (34%)
  local copies, waits for them, and re-layouts  16.5 us (7%)
  matrix products  13.4 us (6%)
  starting transfers between devices  9.53 us (4%)
    all_to_all x1, blocking collectives, exchange(): lax.all_to_all(blocks, ('ep', 'tp'), split_axis=0, concat_axis=0, tiled=T...  107 us
    all_to_all x1, waiting for transfers between devices, exchange(): lax.all_to_all(blocks, ('ep', 'tp'), split_axis=0, concat_axis=0, tiled=T...  75.6 us
    all_to_all x1, starting transfers between devices, exchange(): lax.all_to_all(blocks, ('ep', 'tp'), split_axis=0, concat_axis=0, tiled=T...  9.53 us
    reshape x2, local copies, waits for them, and re-layouts, exchange(): blocks = rows.reshape(experts, capacity * model_width // LANES, LANES)  7.52 us
    reshape x2, local copies, waits for them, and re-layouts, exchange(): return moved.reshape(experts * capacity, model_width)  7.39 us
    dot_general x1, matrix products, on_device(): jnp.dot(hidden, w_down[0], preferred_element_type=jnp.float32)  5.13 us
  transfers between devices with their start and end apart: 1, of which 1 were waited for; matrix products, arithmetic and copies ran while one was open for 0% of the time, Pallas kernels for 0%

profile of v1, /device:TPU:33, one launch (start us, length us, event | category | flops | bytes accessed | tf_op | source)
XLA Modules:
  0.0 222.5 jit_solution(9909879412015605143)
XLA Ops:
  0.0 0.8 slice_bitcast_fusion.2
  0.9 0.1 fusion.33
  1.0 0.1 and.50
  1.1 0.1 and.51
  1.3 0.1 eq.95
  1.4 0.2 eq.97
  1.6 0.0 copy-done.2
  1.6 0.2 fusion.13
  1.8 1.8 convolution_convert_fusion.1
  3.6 3.8 %reshape.169 = bf16[128,48,128]{2,1,0:T(8,128)(2,1)} reshape(bf16[384,2048]{1,0:T(8,128)(2,1)} %convolution_convert_fusion.1) | data formatting | bytes 3145728 | tf_op jit(solution)/shard_map/reshape | solution.py:36
  7.3 107.0 %all_to_all.10 = bf16[128,48,128]{2,1,0:T(8,128)(2,1)} all-to-all(bf16[128,48,128]{2,1,0:T(8,128)(2,1)} %reshape.169), channel_id=1, replica_groups=mesh['grp'=2,'ep'=32,'tp'=4] {'ep','tp'}, dimensions={0} | all-to-all | bytes 3145728 | tf_op jit(solution)/shard_map/all_to_all | solution.py:37
  114.4 3.7 %reshape.170 = bf16[384,2048]{1,0:T(8,128)(2,1)} reshape(bf16[128,48,128]{2,1,0:T(8,128)(2,1)} %all_to_all.10) | data formatting | bytes 3145728 | tf_op jit(solution)/shard_map/reshape | solution.py:38
  118.1 3.0 %fusion.5 = f32[384,512]{1,0:T(8,128)S(1)} fusion(bf16[384,2048]{1,0:T(8,128)(2,1)} %reshape.170, bf16[1,2048,512]{2,1,0:T(8,128)(2,1)} %param.11), kind=kOutput, calls=%fused_computation.9 | convolution fusion | flops 805306368 | bytes 4456448 | tf_op jit(solution)/shard_map/dot_general | solution.py:41
  121.1 0.0 copy-done
  121.1 5.1 %convolution_convert_fusion = bf16[384,2048]{1,0:T(8,128)(2,1)} fusion(bf16[1,512,2048]{2,1,0:T(8,128)(2,1)S(1)} %copy-done, bf16[384,2048]{1,0:T(8,128)(2,1)} %reshape.170, bf16[1,2048,512]{2,1,0:T(8,128)(2,1)} %param.12, f32[384,512]{1,0:T(8,128)S(1)} %fusion.5), kind=kOutput, calls=%fused_computation | convolution fusion | flops 1612578816 | bytes 8126464 | tf_op jit(solution)/shard_map/dot_general | solution.py:44
  126.3 3.8 %reshape.171 = bf16[128,48,128]{2,1,0:T(8,128)(2,1)} reshape(bf16[384,2048]{1,0:T(8,128)(2,1)} %convolution_convert_fusion) | data formatting | bytes 3145728 | tf_op jit(solution)/shard_map/reshape | solution.py:36
  130.0 9.5 %all-to-all-start.1 = ((bf16[128,48,128]{2,1,0:T(8,128)(2,1)}), bf16[128,48,128]{2,1,0:T(8,128)(2,1)}, u32[]{:S(2)}, u32[]{:S(2)}) async-start(bf16[128,48,128]{2,1,0:T(8,128)(2,1)} %reshape.171), calls=%async_computation.1 | async-start | bytes 3145728 | tf_op jit(solution)/shard_map/all_to_all | solution.py:37
  139.5 0.2 fusion.27
  139.7 0.1 and.49
  139.8 0.1 and.55
  140.0 75.6 %all-to-all-done.1 = bf16[128,48,128]{2,1,0:T(8,128)(2,1)} async-done(((bf16[128,48,128]{2,1,0:T(8,128)(2,1)}), bf16[128,48,128]{2,1,0:T(8,128)(2,1)}, u32[]{:S(2)}, u32[]{:S(2)}) %all-to-all-start.1) | async-done | bytes 1572896 | tf_op jit(solution)/shard_map/all_to_all | solution.py:37
  215.5 3.7 %reshape.172 = bf16[384,2048]{1,0:T(8,128)(2,1)} reshape(bf16[128,48,128]{2,1,0:T(8,128)(2,1)} %all-to-all-done.1) | data formatting | bytes 3145728 | tf_op jit(solution)/shard_map/reshape | solution.py:38
  219.2 2.0 convolution_multiply_fusion.1
  221.2 1.3 fusion.1
  (13 shorter events, 0.1 us)
Async XLA Ops:
  0.0 121.1 %copy-start = (bf16[1,512,2048]{2,1,0:T(8,128)(2,1)S(1)}, bf16[1,512,2048]{2,1,0:T(8,128)(2,1)}, u32[]{:S(2)}) copy-start(bf16[1,512,2048]{2,1,0:T(8,128)(2,1)} %param.13) | copy-start | bytes 6291460
  0.0 1.6 copy-start.2
  0.0 1.8 copy-start.3
  130.0 9.9 %copy-start.4 = (f32[128,2]{0,1:T(2,128)S(1)}, f32[128,2]{0,1:T(2,128)}, u32[]{:S(2)}) copy-start(f32[128,2]{0,1:T(2,128)} %param.10) | copy-start | bytes 3076
  130.0 85.5 %all-to-all-start.1 = ((bf16[128,48,128]{2,1,0:T(8,128)(2,1)}), bf16[128,48,128]{2,1,0:T(8,128)(2,1)}, u32[]{:S(2)}, u32[]{:S(2)}) async-start(bf16[128,48,128]{2,1,0:T(8,128)(2,1)} %reshape.171), calls=%async_computation.1 | async-start | bytes 3145728 | tf_op jit(solution)/shard_map/all_to_all | solution.py:37
  219.2 2.0 copy-start.1

commit v2 on v0

v2 whole, which is shorter than its diff:
```python
import jax
import jax.numpy as jnp
from jax import lax
from jax.experimental import pallas as pl
from jax.experimental.pallas import tpu as pltpu
from jax.sharding import PartitionSpec as P

LANES = 128
AXES = ("ep", "tp")
MIB = 1 << 20
WHOLE = pl.BlockSpec(memory_space=pltpu.VMEM)


def swap_table(tiles):
    n = tiles * tiles
    row = lax.broadcasted_iota(jnp.int32, (n, n), 0)
    column = lax.broadcasted_iota(jnp.int32, (n, n), 1)
    source = lax.rem(row, tiles) * tiles + lax.div(row, tiles)
    return (column == source).astype(jnp.bfloat16)


def spread_rows(table, rows_ref, out_ref):
    n, width = rows_ref.shape
    tiles = width // LANES
    span = tiles * tiles
    for g in range(0, n, 2 * tiles):
        halves = []
        for h in (g, g + tiles):
            pieces = [rows_ref[h : h + tiles, c * LANES : (c + 1) * LANES] for c in range(tiles)]
            halves.append(jnp.concatenate(pieces, 0))
        both = jnp.dot(table, jnp.concatenate(halves, 1), preferred_element_type=jnp.float32)
        both = both.astype(jnp.bfloat16)
        out_ref[g * tiles : g * tiles + span, :] = both[:, :LANES]
        out_ref[g * tiles + span : g * tiles + 2 * span, :] = both[:, LANES:]


def gather_rows(table, in_ref, rows_ref):
    n, width = rows_ref.shape
    tiles = width // LANES
    span = tiles * tiles
    for g in range(0, n, 2 * tiles):
        first = in_ref[g * tiles : g * tiles + span, :]
        second = in_ref[g * tiles + span : g * tiles + 2 * span, :]
        both = jnp.dot(
            table, jnp.concatenate([first, second], 1), preferred_element_type=jnp.float32
        ).astype(jnp.bfloat16)
        for c in range(tiles):
            part = both[c * tiles : (c + 1) * tiles]
            rows_ref[g : g + tiles, c * LANES : (c + 1) * LANES] = part[:, :LANES]
            rows_ref[g + tiles : g + 2 * tiles, c * LANES : (c + 1) * LANES] = part[:, LANES:]


def dispatch_kernel(capacity, tokens_ref, gain_ref, ids_ref, out_ref, rows_ref):
    tok_rows, width = tokens_ref.shape
    top_count = ids_ref.shape[0]
    n = rows_ref.shape[0]
    values = tokens_ref[...].astype(jnp.float32)
    scale = lax.rsqrt(jnp.mean(values * values, axis=-1, keepdims=True) + 1e-06)
    normed = (values * scale * gain_ref[...]).astype(jnp.bfloat16)
    row = lax.broadcasted_iota(jnp.int32, (n, tok_rows), 0)
    expert = lax.div(row, capacity)
    named = ids_ref[0:1, :] == expert
    for k in range(1, top_count):
        named = named | (ids_ref[k : k + 1, :] == expert)
    before = lax.broadcasted_iota(jnp.int32, (tok_rows, tok_rows), 0)
    after = lax.broadcasted_iota(jnp.int32, (tok_rows, tok_rows), 1)
    earlier = (before < after).astype(jnp.bfloat16)
    rank = jnp.dot(named.astype(jnp.bfloat16), earlier, preferred_element_type=jnp.float32)
    slot = lax.rem(row, capacity).astype(jnp.float32)
    table = (named & (rank == slot)).astype(jnp.bfloat16)
    rows_ref[...] = jnp.dot(table, normed, preferred_element_type=jnp.float32).astype(jnp.bfloat16)
    spread_rows(swap_table(width // LANES), rows_ref, out_ref)


def picks_kernel(capacity, ids_ref, *out_refs):
    tok_rows = ids_ref.shape[0]
    n = out_refs[0].shape[1]
    row = lax.broadcasted_iota(jnp.int32, (tok_rows, n), 1)
    expert = lax.div(row, capacity)
    picks = [ids_ref[:, k : k + 1] == expert for k in range(len(out_refs))]
    named = picks[0]
    for pick in picks[1:]:
        named = named | pick
    after = lax.broadcasted_iota(jnp.int32, (tok_rows, tok_rows), 0)
    before = lax.broadcasted_iota(jnp.int32, (tok_rows, tok_rows), 1)
    earlier = (before < after).astype(jnp.bfloat16)
    rank = jnp.dot(earlier, named.astype(jnp.bfloat16), preferred_element_type=jnp.float32)
    in_slot = rank == lax.rem(row, capacity).astype(jnp.float32)
    for pick, out_ref in zip(picks, out_refs):
        out_ref[...] = (pick & in_slot).astype(jnp.bfloat16)


def products_kernel(in_ref, gate_ref, up_ref, down_ref, out_ref, rows_ref, hidden_ref):
    width, hidden_width = gate_ref.shape
    table = swap_table(width // LANES)
    gather_rows(table, in_ref, rows_ref)
    rows = rows_ref[...]
    step = 256
    for f in range(0, hidden_width, step):
        gate_act = jnp.dot(rows, gate_ref[:, f : f + step], preferred_element_type=jnp.float32)
        up_act = jnp.dot(rows, up_ref[:, f : f + step], preferred_element_type=jnp.float32)
        hidden_ref[:, f : f + step] = (jax.nn.silu(gate_act) * up_act).astype(jnp.bfloat16)
    hidden = hidden_ref[...]
    for d in range(0, width, step):
        part = jnp.dot(hidden, down_ref[:, d : d + step], preferred_element_type=jnp.float32)
        rows_ref[:, d : d + step] = part.astype(jnp.bfloat16)
    spread_rows(table, rows_ref, out_ref)


def mix_kernel(in_ref, weights_ref, *refs):
    *pick_refs, out_ref, rows_ref = refs
    width = out_ref.shape[1]
    gather_rows(swap_table(width // LANES), in_ref, rows_ref)
    step = 512
    for d in range(0, width, step):
        total = None
        for k, pick_ref in enumerate(pick_refs):
            picked = jnp.dot(
                pick_ref[...], rows_ref[:, d : d + step], preferred_element_type=jnp.float32
            )
            term = picked * weights_ref[:, k : k + 1]
            total = term if total is None else total + term
        out_ref[:, d : d + step] = total.astype(out_ref.dtype)


def on_device(tokens, norm_gain, route_ids, route_weights, w_gate, w_up, w_down):
    tok_rows, width = tokens.shape
    top_count = route_ids.shape[1]
    hidden_width = w_gate.shape[2]
    experts = lax.axis_size("ep") * lax.axis_size("tp")
    capacity = 3 * tok_rows * top_count // (2 * experts)
    n = experts * capacity
    tiles = width // LANES
    flat = jax.ShapeDtypeStruct((n * tiles, LANES), jnp.bfloat16)
    rows_scratch = pltpu.VMEM((n, width), jnp.bfloat16)

    def call(kernel, out_shape, inputs, scratch, name, flops, mib):
        many = isinstance(out_shape, (list, tuple))
        return pl.pallas_call(
            kernel,
            out_shape=out_shape,
            in_specs=[WHOLE] * len(inputs),
            out_specs=[WHOLE] * len(out_shape) if many else WHOLE,
            scratch_shapes=scratch,
            name=name,
            cost_estimate=pl.CostEstimate(flops=flops, bytes_accessed=4 * MIB, transcendentals=0),
            compiler_params=pltpu.CompilerParams(vmem_limit_bytes=mib * MIB),
        )(*inputs)

    def exchange(rows):
        blocks = rows.reshape(experts, capacity * tiles, LANES)
        moved = lax.all_to_all(blocks, AXES, split_axis=0, concat_axis=0, tiled=True)
        return moved.reshape(n * tiles, LANES)

    sent = call(
        lambda *refs: dispatch_kernel(capacity, *refs),
        flat,
        [tokens, norm_gain.reshape(1, width), route_ids.T],
        [rows_scratch],
        "dispatch",
        2 * n * tok_rows * width,
        20,
    )
    received = exchange(sent)
    pick_shape = jax.ShapeDtypeStruct((tok_rows, n), jnp.bfloat16)
    picks = call(
        lambda *refs: picks_kernel(capacity, *refs),
        [pick_shape] * top_count,
        [route_ids],
        [],
        "picks",
        2 * n * tok_rows * tok_rows,
        8,
    )
    result = call(
        products_kernel,
        flat,
        [received, w_gate[0], w_up[0], w_down[0]],
        [rows_scratch, pltpu.VMEM((n, hidden_width), jnp.bfloat16)],
        "products",
        6 * n * width * hidden_width,
        28,
    )
    returned = exchange(result)
    return call(
        mix_kernel,
        jax.ShapeDtypeStruct(tokens.shape, tokens.dtype),
        [returned, route_weights, *picks],
        [rows_scratch],
        "mix",
        2 * top_count * n * tok_rows * width,
        20,
    )


def solution(mesh):
    return jax.shard_map(
        on_device,
        mesh=mesh,
        in_specs=(
            P(("grp", "ep", "tp"), None),
            P(),
            P(("grp", "ep", "tp"), None),
            P(("grp", "ep", "tp"), None),
            P(("ep", "tp"), None, None),
            P(("ep", "tp"), None, None),
            P(("ep", "tp"), None, None),
        ),
        out_specs=P(("grp", "ep", "tp"), None),
        check_vma=False,
    )
```

time: 329 us -> 205 us (0.62)
  local copies, waits for them, and re-layouts: 73.5 us -> 4.25 us
  waiting for transfers between devices: 97.8 us -> 75.4 us
  blocking collectives: 129 us -> 107 us
  Pallas kernels: 0 us -> 8.28 us
  matrix products: 8.19 us -> 0 us
  other arithmetic: 8.17 us -> 0 us
    scatter x2 -> x0, local copies, waits for them, and re-layouts: 47.5 us -> none  [on_device(): buffer = buffer.at[flat_ids, slot_index].set(normed[token_of])]
    all_to_all x1, waiting for transfers between devices: 97.8 us -> 75.4 us  [exchange(): lax.all_to_all(blocks, AXES, split_axis=0, concat_axis=0, tiled=True)]
    all_to_all x1, blocking collectives: 129 us -> 107 us  [exchange(): lax.all_to_all(blocks, AXES, split_axis=0, concat_axis=0, tiled=True)]
    reshape x3 -> x0, local copies, waits for them, and re-layouts: 10.4 us -> none  [the longest x1 5.17 us: on_device(): result.reshape(received.shape)]
    pallas_call x0 -> x4, Pallas kernels: none -> 8.28 us  [call(): pl.pallas_call(kernel, out_shape=out_shape, in_specs=[WHOLE] * len(inputs...]
    dot_general x2 -> x0, matrix products: 8.19 us -> none  [the longest x1 5.15 us: on_device(): jnp.dot(hidden, w_down[0], preferred_element_type=jnp.float32)]
    reduce_sum x3 -> x0, other arithmetic: 7 us -> none  [the longest x1 5.59 us: on_device(): jnp.sum(picked * route_weights[:, :, None], axis=1).astype(jnp.bfloat16)]
    gather x2 -> x0, local copies, waits for them, and re-layouts: 6.47 us -> none  [the longest x1 4.15 us: on_device(): returned[flat_ids, slot_index].reshape(tok_rows, top_count, model_width)]
where the time goes in v2:
time: 205 us; the launch traced here: 204 us
  blocking collectives  107 us (52%)
  waiting for transfers between devices  75.4 us (37%)
  starting transfers between devices  9.47 us (5%)
  Pallas kernels  8.28 us (4%)
  local copies, waits for them, and re-layouts  4.25 us (2%)
    all_to_all x1, blocking collectives, exchange(): lax.all_to_all(blocks, AXES, split_axis=0, concat_axis=0, tiled=True)  107 us
    all_to_all x1, waiting for transfers between devices, exchange(): lax.all_to_all(blocks, AXES, split_axis=0, concat_axis=0, tiled=True)  75.4 us
    all_to_all x1, starting transfers between devices, exchange(): lax.all_to_all(blocks, AXES, split_axis=0, concat_axis=0, tiled=True)  9.47 us
    pallas_call x4, Pallas kernels, call(): pl.pallas_call(kernel, out_shape=out_shape, in_specs=[WHOLE] * len(inputs...  8.28 us
    unnamed x18, local copies, waits for them, and re-layouts  4.25 us
  transfers between devices with their start and end apart: 1, of which 1 were waited for; matrix products, arithmetic and copies ran while one was open for 0% of the time, Pallas kernels for 0%

profile of v2, /device:TPU:33, one launch (start us, length us, event | category | flops | bytes accessed | tf_op | source)
XLA Modules:
  0.0 204.3 jit_solution(8521498002314195945)
XLA Ops:
  0.0 0.0 copy-start.3
  0.0 1.0 copy-done.3
  1.0 0.0 copy-start.4
  1.0 0.7 copy-done.4
  1.7 0.0 copy-start.5
  1.7 0.7 copy-done.5
  2.4 0.0 copy-start.1
  2.4 1.3 dispatch.1
  3.7 0.0 copy-start
  3.7 106.9 %all_to_all.10 = bf16[128,48,128]{2,1,0:T(8,128)(2,1)S(1)} all-to-all(bf16[128,48,128]{2,1,0:T(8,128)(2,1)S(1)} %bitcast.11), channel_id=1, replica_groups=mesh['grp'=2,'ep'=32,'tp'=4] {'ep','tp'}, dimensions={0} | all-to-all | bytes 3145728 | tf_op jit(solution)/shard_map/all_to_all | solution.py:152
  110.6 0.0 copy-done.1
  110.6 0.0 copy-done
  110.6 0.0 copy-start.2
  110.6 1.6 copy-done.2
  112.2 4.7 %products.1 = bf16[6144,128]{1,0:T(8,128)(2,1)} custom-call(bf16[6144,128]{1,0:T(8,128)(2,1)S(1)} %bitcast.10, bf16[2048,512]{1,0:T(8,128)(2,1)S(1)} %bitcast.12, bf16[2048,512]{1,0:T(8,128)(2,1)S(1)} %bitcast.13, bf16[512,2048]{1,0:T(8,128)(2,1)S(1)} %bitcast.14), custom_call_target="tpu_custom_call" | custom-call | flops 2415919104 | bytes 4194304 | tf_op jit(solution)/shard_map/products/pallas_call | solution.py:139
  116.9 0.0 copy-start.6
  116.9 9.5 %all-to-all-start.1 = ((bf16[128,48,128]{2,1,0:T(8,128)(2,1)}), bf16[128,48,128]{2,1,0:T(8,128)(2,1)S(1)}, u32[]{:S(2)}, u32[]{:S(2)}) async-start(bf16[128,48,128]{2,1,0:T(8,128)(2,1)} %bitcast.7), calls=%async_computation.1 | async-start | bytes 3145728 | tf_op jit(solution)/shard_map/all_to_all | solution.py:152
  126.3 0.0 copy-done.6
  126.4 0.1 copy.8.refs_0_
  126.5 0.0 copy-done.7
  126.5 0.1 copy.9.weights_ref
  126.6 0.3 picks.1
  126.9 75.4 %all-to-all-done.1 = bf16[128,48,128]{2,1,0:T(8,128)(2,1)S(1)} async-done(((bf16[128,48,128]{2,1,0:T(8,128)(2,1)}), bf16[128,48,128]{2,1,0:T(8,128)(2,1)S(1)}, u32[]{:S(2)}, u32[]{:S(2)}) %all-to-all-start.1) | async-done | bytes 1572896 | tf_op jit(solution)/shard_map/all_to_all | solution.py:152
  202.3 2.0 mix.1
  (1 shorter events, 0.0 us)
Async XLA Ops:
  0.0 1.0 copy-start.3
  1.0 0.7 copy-start.4
  1.7 0.7 copy-start.5
  2.4 108.2 %copy-start.1 = (bf16[1,2048,512]{2,1,0:T(8,128)(2,1)S(1)}, bf16[1,2048,512]{2,1,0:T(8,128)(2,1)}, u32[]{:S(2)}) copy-start(bf16[1,2048,512]{2,1,0:T(8,128)(2,1)} %param.12) | copy-start | bytes 6291460
  3.7 106.9 %copy-start = (bf16[1,2048,512]{2,1,0:T(8,128)(2,1)S(1)}, bf16[1,2048,512]{2,1,0:T(8,128)(2,1)}, u32[]{:S(2)}) copy-start(bf16[1,2048,512]{2,1,0:T(8,128)(2,1)} %param.11) | copy-start | bytes 6291460
  110.6 1.6 copy-start.2
  116.9 9.5 %copy-start.6 = (s32[128,2]{0,1:T(2,128)S(1)}, s32[128,2]{0,1:T(2,128)}, u32[]{:S(2)}) copy-start(s32[128,2]{0,1:T(2,128)} %param.9) | copy-start | bytes 3076
  116.9 9.6 %copy-start.7 = (f32[128,2]{0,1:T(2,128)S(1)}, f32[128,2]{0,1:T(2,128)}, u32[]{:S(2)}) copy-start(f32[128,2]{0,1:T(2,128)} %param.10) | copy-start | bytes 3076
  116.9 85.4 %all-to-all-start.1 = ((bf16[128,48,128]{2,1,0:T(8,128)(2,1)}), bf16[128,48,128]{2,1,0:T(8,128)(2,1)S(1)}, u32[]{:S(2)}, u32[]{:S(2)}) async-start(bf16[128,48,128]{2,1,0:T(8,128)(2,1)} %bitcast.7), calls=%async_computation.1 | async-start | bytes 3145728 | tf_op jit(solution)/shard_map/all_to_all | solution.py:152

commit v3 on v2

--- a/solution.py
+++ b/solution.py
@@ -9,6 +9,7 @@
 AXES = ("ep", "tp")
 MIB = 1 << 20
 WHOLE = pl.BlockSpec(memory_space=pltpu.VMEM)
+OUTSIDE = pl.BlockSpec(memory_space=pltpu.HBM)
 
 
 def swap_table(tiles):
@@ -19,7 +20,7 @@
     return (column == source).astype(jnp.bfloat16)
 
 
-def spread_rows(table, rows_ref, out_ref):
+def spread_rows(table, rows_ref, out_ref, done=None, parts=1):
     n, width = rows_ref.shape
     tiles = width // LANES
     span = tiles * tiles
@@ -32,6 +33,9 @@
         both = both.astype(jnp.bfloat16)
         out_ref[g * tiles : g * tiles + span, :] = both[:, :LANES]
         out_ref[g * tiles + span : g * tiles + 2 * span, :] = both[:, LANES:]
+        part = n // parts
+        if done is not None and (g + 2 * tiles) % part == 0:
+            done((g + 2 * tiles - part) * tiles, (g + 2 * tiles) * tiles)
 
 
 def gather_rows(table, in_ref, rows_ref):
@@ -50,7 +54,7 @@
             rows_ref[g + tiles : g + 2 * tiles, c * LANES : (c + 1) * LANES] = part[:, LANES:]
 
 
-def dispatch_kernel(capacity, tokens_ref, gain_ref, ids_ref, out_ref, rows_ref):
+def dispatch_kernel(capacity, tokens_ref, gain_ref, ids_ref, rows_ref):
     tok_rows, width = tokens_ref.shape
     top_count = ids_ref.shape[0]
     n = rows_ref.shape[0]
@@ -69,7 +73,10 @@
     slot = lax.rem(row, capacity).astype(jnp.float32)
     table = (named & (rank == slot)).astype(jnp.bfloat16)
     rows_ref[...] = jnp.dot(table, normed, preferred_element_type=jnp.float32).astype(jnp.bfloat16)
-    spread_rows(swap_table(width // LANES), rows_ref, out_ref)
+
+
+def spread_kernel(rows_ref, out_ref):
+    spread_rows(swap_table(rows_ref.shape[1] // LANES), rows_ref, out_ref)
 
 
 def picks_kernel(capacity, ids_ref, *out_refs):
@@ -90,7 +97,9 @@
         out_ref[...] = (pick & in_slot).astype(jnp.bfloat16)
 
 
-def products_kernel(in_ref, gate_ref, up_ref, down_ref, out_ref, rows_ref, hidden_ref):
+def products_kernel(
+    in_ref, gate_ref, up_ref, down_ref, out_hbm, rows_ref, hidden_ref, out_ref, sems
+):
     width, hidden_width = gate_ref.shape
     table = swap_table(width // LANES)
     gather_rows(table, in_ref, rows_ref)
@@ -104,23 +113,40 @@
     for d in range(0, width, step):
         part = jnp.dot(hidden, down_ref[:, d : d + step], preferred_element_type=jnp.float32)
         rows_ref[:, d : d + step] = part.astype(jnp.bfloat16)
-    spread_rows(table, rows_ref, out_ref)
+    copies = []
+
+    def send(first, last):
+        part = slice(first, last)
+        copy = pltpu.make_async_copy(out_ref.at[part], out_hbm.at[part], sems.at[len(copies)])
+        copy.start()
+        copies.append(copy)
+
+    spread_rows(table, rows_ref, out_ref, send, sems.shape[0])
+    for copy in copies:
+        copy.wait()
 
 
 def mix_kernel(in_ref, weights_ref, *refs):
-    *pick_refs, out_ref, rows_ref = refs
-    width = out_ref.shape[1]
+    *pick_refs, out_hbm, rows_ref, mixed_ref, sems = refs
+    width = mixed_ref.shape[1]
     gather_rows(swap_table(width // LANES), in_ref, rows_ref)
-    step = 512
-    for d in range(0, width, step):
+    step = width // sems.shape[0]
+    copies = []
+    for i in range(sems.shape[0]):
+        columns = slice(i * step, (i + 1) * step)
         total = None
         for k, pick_ref in enumerate(pick_refs):
             picked = jnp.dot(
-                pick_ref[...], rows_ref[:, d : d + step], preferred_element_type=jnp.float32
+                pick_ref[...], rows_ref[:, columns], preferred_element_type=jnp.float32
             )
             term = picked * weights_ref[:, k : k + 1]
             total = term if total is None else total + term
-        out_ref[:, d : d + step] = total.astype(out_ref.dtype)
+        mixed_ref[:, columns] = total.astype(mixed_ref.dtype)
+        copy = pltpu.make_async_copy(mixed_ref.at[:, columns], out_hbm.at[:, columns], sems.at[i])
+        copy.start()
+        copies.append(copy)
+    for copy in copies:
+        copy.wait()
 
 
 def on_device(tokens, norm_gain, route_ids, route_weights, w_gate, w_up, w_down):
@@ -134,13 +160,13 @@
     flat = jax.ShapeDtypeStruct((n * tiles, LANES), jnp.bfloat16)
     rows_scratch = pltpu.VMEM((n, width), jnp.bfloat16)
 
-    def call(kernel, out_shape, inputs, scratch, name, flops, mib):
+    def call(kernel, out_shape, inputs, scratch, name, flops, mib, outside=(), out_spec=WHOLE):
         many = isinstance(out_shape, (list, tuple))
         return pl.pallas_call(
             kernel,
             out_shape=out_shape,
-            in_specs=[WHOLE] * len(inputs),
-            out_specs=[WHOLE] * len(out_shape) if many else WHOLE,
+            in_specs=[OUTSIDE if i in outside else WHOLE for i in range(len(inputs))],
+            out_specs=[out_spec] * len(out_shape) if many else out_spec,
             scratch_shapes=scratch,
             name=name,
             cost_estimate=pl.CostEstimate(flops=flops, bytes_accessed=4 * MIB, transcendentals=0),
@@ -152,15 +178,16 @@
         moved = lax.all_to_all(blocks, AXES, split_axis=0, concat_axis=0, tiled=True)
         return moved.reshape(n * tiles, LANES)
 
-    sent = call(
+    rows = call(
         lambda *refs: dispatch_kernel(capacity, *refs),
-        flat,
+        jax.ShapeDtypeStruct((n, width), jnp.bfloat16),
         [tokens, norm_gain.reshape(1, width), route_ids.T],
-        [rows_scratch],
+        [],
         "dispatch",
         2 * n * tok_rows * width,
-        20,
-    )
+        16,
+    )
+    sent = call(spread_kernel, flat, [rows], [], "spread", 2 * n * 256 * width, 16)
     received = exchange(sent)
     pick_shape = jax.ShapeDtypeStruct((tok_rows, n), jnp.bfloat16)
     picks = call(
@@ -176,20 +203,31 @@
         products_kernel,
         flat,
         [received, w_gate[0], w_up[0], w_down[0]],
-        [rows_scratch, pltpu.VMEM((n, hidden_width), jnp.bfloat16)],
+        [
+            rows_scratch,
+            pltpu.VMEM((n, hidden_width), jnp.bfloat16),
+            pltpu.VMEM(flat.shape, flat.dtype),
+            pltpu.SemaphoreType.DMA((4,)),
+        ],
         "products",
         6 * n * width * hidden_width,
         28,
+        out_spec=OUTSIDE,
     )
     returned = exchange(result)
     return call(
         mix_kernel,
         jax.ShapeDtypeStruct(tokens.shape, tokens.dtype),
         [returned, route_weights, *picks],
-        [rows_scratch],
+        [
+            rows_scratch,
+            pltpu.VMEM(tokens.shape, tokens.dtype),
+            pltpu.SemaphoreType.DMA((4,)),
+        ],
         "mix",
         2 * top_count * n * tok_rows * width,
         20,
+        out_spec=OUTSIDE,
     )
 
 

time: 205 us -> 203 us (level)
    pallas_call x4 -> x5, Pallas kernels: 8.28 us -> 8.02 us  [call(): pl.pallas_call(kernel, out_shape=out_shape, in_specs=[OUTSIDE if i in out...]
where the time goes in v3:
time: 203 us
  blocking collectives  107 us (53%)
  waiting for transfers between devices  75.4 us (37%)
  starting transfers between devices  9.35 us (5%)
  Pallas kernels  8.02 us (4%)
  local copies, waits for them, and re-layouts  2.67 us (1%)
    all_to_all x1, blocking collectives, exchange(): lax.all_to_all(blocks, AXES, split_axis=0, concat_axis=0, tiled=True)  107 us
    all_to_all x1, waiting for transfers between devices, exchange(): lax.all_to_all(blocks, AXES, split_axis=0, concat_axis=0, tiled=True)  75.4 us
    all_to_all x1, starting transfers between devices, exchange(): lax.all_to_all(blocks, AXES, split_axis=0, concat_axis=0, tiled=True)  9.35 us
    pallas_call x5, Pallas kernels, call(): pl.pallas_call(kernel, out_shape=out_shape, in_specs=[OUTSIDE if i in out...  8.02 us
  transfers between devices with their start and end apart: 1, of which 1 were waited for; matrix products, arithmetic and copies ran while one was open for 0% of the time, Pallas kernels for 0%

profile of v3, /device:TPU:33, one launch (start us, length us, event | category | flops | bytes accessed | tf_op | source)
XLA Modules:
  0.0 202.5 jit_solution(8517968474602320951)
XLA Ops:
  0.0 0.0 copy-start.3
  0.0 1.0 copy-done.3
  1.0 0.7 copy-done.4
  1.7 0.7 copy-done.5
  2.4 0.8 dispatch.1.rows_ref
  3.2 0.0 copy-start.1
  3.2 0.0 copy-start.2
  3.2 0.6 spread.1
  3.8 0.0 copy-start
  3.8 107.0 %all_to_all.10 = bf16[128,48,128]{2,1,0:T(8,128)(2,1)S(1)} all-to-all(bf16[128,48,128]{2,1,0:T(8,128)(2,1)S(1)} %bitcast.10), channel_id=1, replica_groups=mesh['grp'=2,'ep'=32,'tp'=4] {'ep','tp'}, dimensions={0} | all-to-all | bytes 3145728 | tf_op jit(solution)/shard_map/all_to_all | solution.py:178
  110.8 0.0 copy-done.1
  110.8 0.0 copy-done.2
  110.8 0.0 copy-done
  110.8 4.5 %products.1 = bf16[6144,128]{1,0:T(8,128)(2,1)} custom-call(bf16[6144,128]{1,0:T(8,128)(2,1)S(1)} %bitcast.11, bf16[2048,512]{1,0:T(8,128)(2,1)S(1)} %bitcast.12, bf16[2048,512]{1,0:T(8,128)(2,1)S(1)} %bitcast.13, bf16[512,2048]{1,0:T(8,128)(2,1)S(1)} %bitcast.14), custom_call_target="tpu_custom_call" | custom-call | flops 2415919104 | bytes 4194304 | tf_op jit(solution)/shard_map/products/pallas_call | solution.py:165
  115.3 0.0 copy-start.6
  115.3 0.0 copy-start.7
  115.3 9.3 %all-to-all-start.1 = ((bf16[128,48,128]{2,1,0:T(8,128)(2,1)}), bf16[128,48,128]{2,1,0:T(8,128)(2,1)S(1)}, u32[]{:S(2)}, u32[]{:S(2)}) async-start(bf16[128,48,128]{2,1,0:T(8,128)(2,1)} %bitcast.7), calls=%async_computation.1 | async-start | bytes 3145728 | tf_op jit(solution)/shard_map/all_to_all | solution.py:178
  124.7 0.0 copy-done.6
  124.7 0.1 copy.8.refs_0_
  124.8 0.0 copy-done.7
  124.8 0.1 copy.9.weights_ref
  124.9 0.3 picks.1
  125.2 75.4 %all-to-all-done.1 = bf16[128,48,128]{2,1,0:T(8,128)(2,1)S(1)} async-done(((bf16[128,48,128]{2,1,0:T(8,128)(2,1)}), bf16[128,48,128]{2,1,0:T(8,128)(2,1)S(1)}, u32[]{:S(2)}, u32[]{:S(2)}) %all-to-all-start.1) | async-done | bytes 1572896 | tf_op jit(solution)/shard_map/all_to_all | solution.py:178
  200.6 1.9 mix.1
  (2 shorter events, 0.0 us)
Async XLA Ops:
  0.0 1.0 copy-start.3
  1.0 0.7 copy-start.4
  1.7 0.7 copy-start.5
  3.2 107.6 %copy-start.1 = (bf16[1,2048,512]{2,1,0:T(8,128)(2,1)S(1)}, bf16[1,2048,512]{2,1,0:T(8,128)(2,1)}, u32[]{:S(2)}) copy-start(bf16[1,2048,512]{2,1,0:T(8,128)(2,1)} %param.12) | copy-start | bytes 6291460
  3.2 107.6 %copy-start.2 = (bf16[1,512,2048]{2,1,0:T(8,128)(2,1)S(1)}, bf16[1,512,2048]{2,1,0:T(8,128)(2,1)}, u32[]{:S(2)}) copy-start(bf16[1,512,2048]{2,1,0:T(8,128)(2,1)} %param.13) | copy-start | bytes 6291460
  3.8 107.0 %copy-start = (bf16[1,2048,512]{2,1,0:T(8,128)(2,1)S(1)}, bf16[1,2048,512]{2,1,0:T(8,128)(2,1)}, u32[]{:S(2)}) copy-start(bf16[1,2048,512]{2,1,0:T(8,128)(2,1)} %param.11) | copy-start | bytes 6291460
  115.3 9.4 %copy-start.6 = (s32[128,2]{0,1:T(2,128)S(1)}, s32[128,2]{0,1:T(2,128)}, u32[]{:S(2)}) copy-start(s32[128,2]{0,1:T(2,128)} %param.9) | copy-start | bytes 3076
  115.3 9.5 %copy-start.7 = (f32[128,2]{0,1:T(2,128)S(1)}, f32[128,2]{0,1:T(2,128)}, u32[]{:S(2)}) copy-start(f32[128,2]{0,1:T(2,128)} %param.10) | copy-start | bytes 3076
  115.3 85.3 %all-to-all-start.1 = ((bf16[128,48,128]{2,1,0:T(8,128)(2,1)}), bf16[128,48,128]{2,1,0:T(8,128)(2,1)S(1)}, u32[]{:S(2)}, u32[]{:S(2)}) async-start(bf16[128,48,128]{2,1,0:T(8,128)(2,1)} %bitcast.7), calls=%async_computation.1 | async-start | bytes 3145728 | tf_op jit(solution)/shard_map/all_to_all | solution.py:178

commit v4 on v3

--- a/solution.py
+++ b/solution.py
@@ -8,16 +8,17 @@
 LANES = 128
 AXES = ("ep", "tp")
 MIB = 1 << 20
+AHEAD = 1 << 32
 WHOLE = pl.BlockSpec(memory_space=pltpu.VMEM)
 OUTSIDE = pl.BlockSpec(memory_space=pltpu.HBM)
 
 
-def swap_table(tiles):
+def swap_kernel(tiles, out_ref):
     n = tiles * tiles
     row = lax.broadcasted_iota(jnp.int32, (n, n), 0)
     column = lax.broadcasted_iota(jnp.int32, (n, n), 1)
     source = lax.rem(row, tiles) * tiles + lax.div(row, tiles)
-    return (column == source).astype(jnp.bfloat16)
+    out_ref[...] = (column == source).astype(jnp.bfloat16)
 
 
 def spread_rows(table, rows_ref, out_ref, done=None, parts=1):
@@ -54,29 +55,31 @@
             rows_ref[g + tiles : g + 2 * tiles, c * LANES : (c + 1) * LANES] = part[:, LANES:]
 
 
-def dispatch_kernel(capacity, tokens_ref, gain_ref, ids_ref, rows_ref):
-    tok_rows, width = tokens_ref.shape
-    top_count = ids_ref.shape[0]
-    n = rows_ref.shape[0]
-    values = tokens_ref[...].astype(jnp.float32)
-    scale = lax.rsqrt(jnp.mean(values * values, axis=-1, keepdims=True) + 1e-06)
-    normed = (values * scale * gain_ref[...]).astype(jnp.bfloat16)
+def table_kernel(capacity, ids_ref, table_ref):
+    n, tok_rows = table_ref.shape
     row = lax.broadcasted_iota(jnp.int32, (n, tok_rows), 0)
     expert = lax.div(row, capacity)
     named = ids_ref[0:1, :] == expert
-    for k in range(1, top_count):
+    for k in range(1, ids_ref.shape[0]):
         named = named | (ids_ref[k : k + 1, :] == expert)
     before = lax.broadcasted_iota(jnp.int32, (tok_rows, tok_rows), 0)
     after = lax.broadcasted_iota(jnp.int32, (tok_rows, tok_rows), 1)
     earlier = (before < after).astype(jnp.bfloat16)
     rank = jnp.dot(named.astype(jnp.bfloat16), earlier, preferred_element_type=jnp.float32)
     slot = lax.rem(row, capacity).astype(jnp.float32)
-    table = (named & (rank == slot)).astype(jnp.bfloat16)
-    rows_ref[...] = jnp.dot(table, normed, preferred_element_type=jnp.float32).astype(jnp.bfloat16)
-
-
-def spread_kernel(rows_ref, out_ref):
-    spread_rows(swap_table(rows_ref.shape[1] // LANES), rows_ref, out_ref)
+    table_ref[...] = (named & (rank == slot)).astype(jnp.bfloat16)
+
+
+def dispatch_kernel(tokens_ref, gain_ref, table_ref, rows_ref):
+    values = tokens_ref[...].astype(jnp.float32)
+    scale = lax.rsqrt(jnp.mean(values * values, axis=-1, keepdims=True) + 1e-06)
+    normed = (values * scale * gain_ref[...]).astype(jnp.bfloat16)
+    rows = jnp.dot(table_ref[...], normed, preferred_element_type=jnp.float32)
+    rows_ref[...] = rows.astype(jnp.bfloat16)
+
+
+def spread_kernel(swap_ref, rows_ref, out_ref):
+    spread_rows(swap_ref[...], rows_ref, out_ref)
 
 
 def picks_kernel(capacity, ids_ref, *out_refs):
@@ -98,10 +101,10 @@
 
 
 def products_kernel(
-    in_ref, gate_ref, up_ref, down_ref, out_hbm, rows_ref, hidden_ref, out_ref, sems
+    swap_ref, in_ref, gate_ref, up_ref, down_ref, out_hbm, rows_ref, hidden_ref, out_ref, sems
 ):
     width, hidden_width = gate_ref.shape
-    table = swap_table(width // LANES)
+    table = swap_ref[...]
     gather_rows(table, in_ref, rows_ref)
     rows = rows_ref[...]
     step = 256
@@ -126,10 +129,10 @@
         copy.wait()
 
 
-def mix_kernel(in_ref, weights_ref, *refs):
+def mix_kernel(swap_ref, in_ref, weights_ref, *refs):
     *pick_refs, out_hbm, rows_ref, mixed_ref, sems = refs
     width = mixed_ref.shape[1]
-    gather_rows(swap_table(width // LANES), in_ref, rows_ref)
+    gather_rows(swap_ref[...], in_ref, rows_ref)
     step = width // sems.shape[0]
     copies = []
     for i in range(sems.shape[0]):
@@ -178,16 +181,34 @@
         moved = lax.all_to_all(blocks, AXES, split_axis=0, concat_axis=0, tiled=True)
         return moved.reshape(n * tiles, LANES)
 
+    swap = call(
+        lambda ref: swap_kernel(tiles, ref),
+        jax.ShapeDtypeStruct((tiles * tiles, tiles * tiles), jnp.bfloat16),
+        [],
+        [],
+        "swap",
+        AHEAD,
+        4,
+    )
+    table = call(
+        lambda *refs: table_kernel(capacity, *refs),
+        jax.ShapeDtypeStruct((n, tok_rows), jnp.bfloat16),
+        [route_ids.T],
+        [],
+        "table",
+        AHEAD,
+        8,
+    )
     rows = call(
-        lambda *refs: dispatch_kernel(capacity, *refs),
+        dispatch_kernel,
         jax.ShapeDtypeStruct((n, width), jnp.bfloat16),
-        [tokens, norm_gain.reshape(1, width), route_ids.T],
+        [tokens, norm_gain.reshape(1, width), table],
         [],
         "dispatch",
         2 * n * tok_rows * width,
         16,
     )
-    sent = call(spread_kernel, flat, [rows], [], "spread", 2 * n * 256 * width, 16)
+    sent = call(spread_kernel, flat, [swap, rows], [], "spread", 2 * n * 256 * width, 16)
     received = exchange(sent)
     pick_shape = jax.ShapeDtypeStruct((tok_rows, n), jnp.bfloat16)
     picks = call(
@@ -202,7 +223,7 @@
     result = call(
         products_kernel,
         flat,
-        [received, w_gate[0], w_up[0], w_down[0]],
+        [swap, received, w_gate[0], w_up[0], w_down[0]],
         [
             rows_scratch,
             pltpu.VMEM((n, hidden_width), jnp.bfloat16),
@@ -218,7 +239,7 @@
     return call(
         mix_kernel,
         jax.ShapeDtypeStruct(tokens.shape, tokens.dtype),
-        [returned, route_weights, *picks],
+        [swap, returned, route_weights, *picks],
         [
             rows_scratch,
             pltpu.VMEM(tokens.shape, tokens.dtype),

time: 203 us -> 202 us (level)
    pallas_call x5 -> x7, Pallas kernels: 8.02 us -> 8.22 us  [call(): pl.pallas_call(kernel, out_shape=out_shape, in_specs=[OUTSIDE if i in out...]
where the time goes in v4:
time: 202 us
  blocking collectives  107 us (53%)
  waiting for transfers between devices  75.4 us (37%)
  starting transfers between devices  9.34 us (5%)
  Pallas kernels  8.22 us (4%)
    all_to_all x1, blocking collectives, exchange(): lax.all_to_all(blocks, AXES, split_axis=0, concat_axis=0, tiled=True)  107 us
    all_to_all x1, waiting for transfers between devices, exchange(): lax.all_to_all(blocks, AXES, split_axis=0, concat_axis=0, tiled=True)  75.4 us
    all_to_all x1, starting transfers between devices, exchange(): lax.all_to_all(blocks, AXES, split_axis=0, concat_axis=0, tiled=True)  9.34 us
    pallas_call x7, Pallas kernels, call(): pl.pallas_call(kernel, out_shape=out_shape, in_specs=[OUTSIDE if i in out...  8.22 us
  transfers between devices with their start and end apart: 1, of which 1 were waited for; matrix products, arithmetic and copies ran while one was open for 0% of the time, Pallas kernels for 0%

profile of v4, /device:TPU:33, one launch (start us, length us, event | category | flops | bytes accessed | tf_op | source)
XLA Modules:
  0.0 201.8 jit_solution(11526197392191744366)
XLA Ops:
  0.0 0.0 copy-start.5
  0.1 0.6 copy-done.5
  0.7 0.0 copy-start.3
  0.7 0.2 table.1.table_ref
  0.9 0.8 copy-done.3
  1.7 0.0 copy-done.4
  1.7 0.7 dispatch.1.rows_ref
  2.5 0.0 copy-start.1
  2.5 0.0 copy-start.2
  2.5 0.6 spread.1
  3.1 0.0 copy-start
  3.1 107.0 %all_to_all.10 = bf16[128,48,128]{2,1,0:T(8,128)(2,1)S(1)} all-to-all(bf16[128,48,128]{2,1,0:T(8,128)(2,1)S(1)} %bitcast.10), channel_id=1, replica_groups=mesh['grp'=2,'ep'=32,'tp'=4] {'ep','tp'}, dimensions={0} | all-to-all | bytes 3145728 | tf_op jit(solution)/shard_map/all_to_all | solution.py:181
  110.1 0.0 copy-done.1
  110.1 0.0 copy-done.2
  110.1 0.0 copy-done
  110.1 4.5 %products.1 = bf16[6144,128]{1,0:T(8,128)(2,1)} custom-call(bf16[256,256]{1,0:T(8,128)(2,1)S(1)} %swap.1.swap_ref, bf16[6144,128]{1,0:T(8,128)(2,1)S(1)} %bitcast.11, bf16[2048,512]{1,0:T(8,128)(2,1)S(1)} %bitcast.12, bf16[2048,512]{1,0:T(8,128)(2,1)S(1)} %bitcast.13, bf16[512,2048]{1,0:T(8,128)(2,1)S(1)} %bitcast.14), custom_call_target="tpu_custom_call" | custom-call | flops 2415919104 | bytes 4194304 | tf_op jit(solution)/shard_map/products/pallas_call | solution.py:168
  114.5 0.0 copy-start.6
  114.6 9.3 %all-to-all-start.1 = ((bf16[128,48,128]{2,1,0:T(8,128)(2,1)}), bf16[128,48,128]{2,1,0:T(8,128)(2,1)S(1)}, u32[]{:S(2)}, u32[]{:S(2)}) async-start(bf16[128,48,128]{2,1,0:T(8,128)(2,1)} %bitcast.7), calls=%async_computation.1 | async-start | bytes 3145728 | tf_op jit(solution)/shard_map/all_to_all | solution.py:181
  123.9 0.1 copy.8.refs_0_
  124.0 0.0 copy-done.6
  124.0 0.1 copy.9.weights_ref
  124.1 0.3 picks.1
  124.4 75.4 %all-to-all-done.1 = bf16[128,48,128]{2,1,0:T(8,128)(2,1)S(1)} async-done(((bf16[128,48,128]{2,1,0:T(8,128)(2,1)}), bf16[128,48,128]{2,1,0:T(8,128)(2,1)S(1)}, u32[]{:S(2)}, u32[]{:S(2)}) %all-to-all-start.1) | async-done | bytes 1572896 | tf_op jit(solution)/shard_map/all_to_all | solution.py:181
  199.8 1.9 mix.1
  (2 shorter events, 0.1 us)
Async XLA Ops:
  0.0 0.7 copy-start.5
  0.7 1.0 copy-start.3
  0.7 1.0 copy-start.4
  2.5 107.6 %copy-start.1 = (bf16[1,2048,512]{2,1,0:T(8,128)(2,1)S(1)}, bf16[1,2048,512]{2,1,0:T(8,128)(2,1)}, u32[]{:S(2)}) copy-start(bf16[1,2048,512]{2,1,0:T(8,128)(2,1)} %param.12) | copy-start | bytes 6291460
  2.5 107.6 %copy-start.2 = (bf16[1,512,2048]{2,1,0:T(8,128)(2,1)S(1)}, bf16[1,512,2048]{2,1,0:T(8,128)(2,1)}, u32[]{:S(2)}) copy-start(bf16[1,512,2048]{2,1,0:T(8,128)(2,1)} %param.13) | copy-start | bytes 6291460
  3.1 107.0 %copy-start = (bf16[1,2048,512]{2,1,0:T(8,128)(2,1)S(1)}, bf16[1,2048,512]{2,1,0:T(8,128)(2,1)}, u32[]{:S(2)}) copy-start(bf16[1,2048,512]{2,1,0:T(8,128)(2,1)} %param.11) | copy-start | bytes 6291460
  114.5 9.5 %copy-start.6 = (f32[128,2]{0,1:T(2,128)S(1)}, f32[128,2]{0,1:T(2,128)}, u32[]{:S(2)}) copy-start(f32[128,2]{0,1:T(2,128)} %param.10) | copy-start | bytes 3076
  114.6 85.3 %all-to-all-start.1 = ((bf16[128,48,128]{2,1,0:T(8,128)(2,1)}), bf16[128,48,128]{2,1,0:T(8,128)(2,1)S(1)}, u32[]{:S(2)}, u32[]{:S(2)}) async-start(bf16[128,48,128]{2,1,0:T(8,128)(2,1)} %bitcast.7), calls=%async_computation.1 | async-start | bytes 3145728 | tf_op jit(solution)/shard_map/all_to_all | solution.py:181

commit v5 on v4

--- a/solution.py
+++ b/solution.py
@@ -21,7 +21,7 @@
     out_ref[...] = (column == source).astype(jnp.bfloat16)
 
 
-def spread_rows(table, rows_ref, out_ref, done=None, parts=1):
+def spread_rows(table, rows_ref, out_ref):
     n, width = rows_ref.shape
     tiles = width // LANES
     span = tiles * tiles
@@ -34,9 +34,6 @@
         both = both.astype(jnp.bfloat16)
         out_ref[g * tiles : g * tiles + span, :] = both[:, :LANES]
         out_ref[g * tiles + span : g * tiles + 2 * span, :] = both[:, LANES:]
-        part = n // parts
-        if done is not None and (g + 2 * tiles) % part == 0:
-            done((g + 2 * tiles - part) * tiles, (g + 2 * tiles) * tiles)
 
 
 def gather_rows(table, in_ref, rows_ref):
@@ -55,53 +52,35 @@
             rows_ref[g + tiles : g + 2 * tiles, c * LANES : (c + 1) * LANES] = part[:, LANES:]
 
 
-def table_kernel(capacity, ids_ref, table_ref):
+def table_kernel(capacity, ids_ref, table_ref, *pick_refs):
     n, tok_rows = table_ref.shape
     row = lax.broadcasted_iota(jnp.int32, (n, tok_rows), 0)
     expert = lax.div(row, capacity)
-    named = ids_ref[0:1, :] == expert
-    for k in range(1, ids_ref.shape[0]):
-        named = named | (ids_ref[k : k + 1, :] == expert)
+    picks = [ids_ref[k : k + 1, :] == expert for k in range(ids_ref.shape[0])]
+    named = picks[0]
+    for pick in picks[1:]:
+        named = named | pick
     before = lax.broadcasted_iota(jnp.int32, (tok_rows, tok_rows), 0)
     after = lax.broadcasted_iota(jnp.int32, (tok_rows, tok_rows), 1)
     earlier = (before < after).astype(jnp.bfloat16)
     rank = jnp.dot(named.astype(jnp.bfloat16), earlier, preferred_element_type=jnp.float32)
-    slot = lax.rem(row, capacity).astype(jnp.float32)
-    table_ref[...] = (named & (rank == slot)).astype(jnp.bfloat16)
-
-
-def dispatch_kernel(tokens_ref, gain_ref, table_ref, rows_ref):
+    in_slot = rank == lax.rem(row, capacity).astype(jnp.float32)
+    table_ref[...] = (named & in_slot).astype(jnp.bfloat16)
+    for pick, pick_ref in zip(picks, pick_refs):
+        pick_ref[...] = (pick & in_slot).astype(jnp.bfloat16)
+
+
+def dispatch_kernel(tokens_ref, gain_ref, table_ref, swap_ref, out_ref, rows_ref):
     values = tokens_ref[...].astype(jnp.float32)
     scale = lax.rsqrt(jnp.mean(values * values, axis=-1, keepdims=True) + 1e-06)
     normed = (values * scale * gain_ref[...]).astype(jnp.bfloat16)
     rows = jnp.dot(table_ref[...], normed, preferred_element_type=jnp.float32)
     rows_ref[...] = rows.astype(jnp.bfloat16)
-
-
-def spread_kernel(swap_ref, rows_ref, out_ref):
     spread_rows(swap_ref[...], rows_ref, out_ref)
 
 
-def picks_kernel(capacity, ids_ref, *out_refs):
-    tok_rows = ids_ref.shape[0]
-    n = out_refs[0].shape[1]
-    row = lax.broadcasted_iota(jnp.int32, (tok_rows, n), 1)
-    expert = lax.div(row, capacity)
-    picks = [ids_ref[:, k : k + 1] == expert for k in range(len(out_refs))]
-    named = picks[0]
-    for pick in picks[1:]:
-        named = named | pick
-    after = lax.broadcasted_iota(jnp.int32, (tok_rows, tok_rows), 0)
-    before = lax.broadcasted_iota(jnp.int32, (tok_rows, tok_rows), 1)
-    earlier = (before < after).astype(jnp.bfloat16)
-    rank = jnp.dot(earlier, named.astype(jnp.bfloat16), preferred_element_type=jnp.float32)
-    in_slot = rank == lax.rem(row, capacity).astype(jnp.float32)
-    for pick, out_ref in zip(picks, out_refs):
-        out_ref[...] = (pick & in_slot).astype(jnp.bfloat16)
-
-
 def products_kernel(
-    swap_ref, in_ref, gate_ref, up_ref, down_ref, out_hbm, rows_ref, hidden_ref, out_ref, sems
+    swap_ref, in_ref, gate_ref, up_ref, down_ref, out_ref, rows_ref, hidden_ref
 ):
     width, hidden_width = gate_ref.shape
     table = swap_ref[...]
@@ -116,33 +95,29 @@
     for d in range(0, width, step):
         part = jnp.dot(hidden, down_ref[:, d : d + step], preferred_element_type=jnp.float32)
         rows_ref[:, d : d + step] = part.astype(jnp.bfloat16)
-    copies = []
-
-    def send(first, last):
-        part = slice(first, last)
-        copy = pltpu.make_async_copy(out_ref.at[part], out_hbm.at[part], sems.at[len(copies)])
-        copy.start()
-        copies.append(copy)
-
-    spread_rows(table, rows_ref, out_ref, send, sems.shape[0])
-    for copy in copies:
-        copy.wait()
+    spread_rows(table, rows_ref, out_ref)
 
 
 def mix_kernel(swap_ref, in_ref, weights_ref, *refs):
     *pick_refs, out_hbm, rows_ref, mixed_ref, sems = refs
     width = mixed_ref.shape[1]
     gather_rows(swap_ref[...], in_ref, rows_ref)
+    top_count, tok_rows = weights_ref.shape
+    padding = jnp.zeros((8 - top_count, tok_rows), jnp.float32)
+    weights = jnp.concatenate([weights_ref[...], padding], 0).T
     step = width // sems.shape[0]
     copies = []
     for i in range(sems.shape[0]):
         columns = slice(i * step, (i + 1) * step)
         total = None
         for k, pick_ref in enumerate(pick_refs):
-            picked = jnp.dot(
-                pick_ref[...], rows_ref[:, columns], preferred_element_type=jnp.float32
+            picked = lax.dot_general(
+                pick_ref[...],
+                rows_ref[:, columns],
+                (((0,), (0,)), ((), ())),
+                preferred_element_type=jnp.float32,
             )
-            term = picked * weights_ref[:, k : k + 1]
+            term = picked * weights[:, k : k + 1]
             total = term if total is None else total + term
         mixed_ref[:, columns] = total.astype(mixed_ref.dtype)
         copy = pltpu.make_async_copy(mixed_ref.at[:, columns], out_hbm.at[:, columns], sems.at[i])
@@ -190,36 +165,25 @@
         AHEAD,
         4,
     )
-    table = call(
+    table, *picks = call(
         lambda *refs: table_kernel(capacity, *refs),
-        jax.ShapeDtypeStruct((n, tok_rows), jnp.bfloat16),
+        [jax.ShapeDtypeStruct((n, tok_rows), jnp.bfloat16)] * (1 + top_count),
         [route_ids.T],
         [],
         "table",
-        AHEAD,
-        8,
-    )
-    rows = call(
-        dispatch_kernel,
-        jax.ShapeDtypeStruct((n, width), jnp.bfloat16),
-        [tokens, norm_gain.reshape(1, width), table],
-        [],
-        "dispatch",
-        2 * n * tok_rows * width,
-        16,
-    )
-    sent = call(spread_kernel, flat, [swap, rows], [], "spread", 2 * n * 256 * width, 16)
-    received = exchange(sent)
-    pick_shape = jax.ShapeDtypeStruct((tok_rows, n), jnp.bfloat16)
-    picks = call(
-        lambda *refs: picks_kernel(capacity, *refs),
-        [pick_shape] * top_count,
-        [route_ids],
-        [],
-        "picks",
         2 * n * tok_rows * tok_rows,
         8,
     )
+    sent = call(
+        dispatch_kernel,
+        flat,
+        [tokens, norm_gain.reshape(1, width), table, swap],
+        [rows_scratch],
+        "dispatch",
+        AHEAD,
+        16,
+    )
+    received = exchange(sent)
     result = call(
         products_kernel,
         flat,
@@ -227,19 +191,16 @@
         [
             rows_scratch,
             pltpu.VMEM((n, hidden_width), jnp.bfloat16),
-            pltpu.VMEM(flat.shape, flat.dtype),
-            pltpu.SemaphoreType.DMA((4,)),
         ],
         "products",
         6 * n * width * hidden_width,
         28,
-        out_spec=OUTSIDE,
     )
     returned = exchange(result)
     return call(
         mix_kernel,
         jax.ShapeDtypeStruct(tokens.shape, tokens.dtype),
-        [swap, returned, route_weights, *picks],
+        [swap, returned, route_weights.T, *picks],
         [
             rows_scratch,
             pltpu.VMEM(tokens.shape, tokens.dtype),

time: 202 us -> 200 us (0.990)
  blocking collectives: 107 us -> 192 us
  waiting for transfers between devices: 75.4 us -> 0 us
  starting transfers between devices: 9.34 us -> 0 us
    all_to_all x1 -> x2, blocking collectives: 107 us -> 192 us  [exchange(): lax.all_to_all(blocks, AXES, split_axis=0, concat_axis=0, tiled=True)]
    all_to_all x1 -> x0, waiting for transfers between devices: 75.4 us -> none  [exchange(): lax.all_to_all(blocks, AXES, split_axis=0, concat_axis=0, tiled=True)]
    all_to_all x1 -> x0, starting transfers between devices: 9.34 us -> none  [exchange(): lax.all_to_all(blocks, AXES, split_axis=0, concat_axis=0, tiled=True)]
    pallas_call x7 -> x5, Pallas kernels: 8.22 us -> 7.01 us  [call(): pl.pallas_call(kernel, out_shape=out_shape, in_specs=[OUTSIDE if i in out...]
  transfers between devices with their start and end apart: 1 -> 0, of which waited for: 1 -> 0; matrix products, arithmetic and copies ran while one was open for 0% -> 0% of each run, Pallas kernels for 0% -> 0%
where the time goes in v5:
time: 200 us
  blocking collectives  192 us (96%)
  Pallas kernels  7.01 us (4%)
    all_to_all x2, blocking collectives, exchange(): lax.all_to_all(blocks, AXES, split_axis=0, concat_axis=0, tiled=True)  192 us
    pallas_call x5, Pallas kernels, call(): pl.pallas_call(kernel, out_shape=out_shape, in_specs=[OUTSIDE if i in out...  7.01 us

profile of v5, /device:TPU:33, one launch (start us, length us, event | category | flops | bytes accessed | tf_op | source)
XLA Modules:
  0.0 199.8 jit_solution(5415521699310945882)
XLA Ops:
  0.0 0.0 copy-start.6
  0.0 0.0 copy-start.5
  0.0 0.0 copy-start.4
  0.1 0.6 copy-done.6
  0.7 0.2 table.1
  0.9 0.0 copy-done.5
  0.9 0.2 copy-done.4
  1.1 0.0 copy-start.1
  1.1 0.0 copy-start.2
  1.1 1.2 dispatch.1
  2.3 0.0 copy-start
  2.3 106.9 %all_to_all.10 = bf16[128,48,128]{2,1,0:T(8,128)(2,1)S(1)} all-to-all(bf16[128,48,128]{2,1,0:T(8,128)(2,1)S(1)} %bitcast.16), channel_id=1, replica_groups=mesh['grp'=2,'ep'=32,'tp'=4] {'ep','tp'}, dimensions={0} | all-to-all | bytes 3145728 | tf_op jit(solution)/shard_map/all_to_all | solution.py:156
  109.2 0.0 copy-done.1
  109.2 0.0 copy-done.2
  109.2 0.0 copy-done
  109.2 3.5 %products.1 = bf16[6144,128]{1,0:T(8,128)(2,1)S(1)} custom-call(bf16[256,256]{1,0:T(8,128)(2,1)S(1)} %swap.1.swap_ref, bf16[6144,128]{1,0:T(8,128)(2,1)S(1)} %bitcast.11, bf16[2048,512]{1,0:T(8,128)(2,1)S(1)} %bitcast.13, bf16[2048,512]{1,0:T(8,128)(2,1)S(1)} %bitcast.14, bf16[512,2048]{1,0:T(8,128)(2,1)S(1)} %bitcast.15), custom_call_target="tpu_custom_call" | custom-call | flops 2415919104 | bytes 4194304 | tf_op jit(solution)/shard_map/products/pallas_call | solution.py:143
  112.7 0.0 copy-start.3
  112.8 85.1 %all_to_all.11 = bf16[128,48,128]{2,1,0:T(8,128)(2,1)S(1)} all-to-all(bf16[128,48,128]{2,1,0:T(8,128)(2,1)S(1)} %bitcast.12), channel_id=1, replica_groups=mesh['grp'=2,'ep'=32,'tp'=4] {'ep','tp'}, dimensions={0} | all-to-all | bytes 3145728 | tf_op jit(solution)/shard_map/all_to_all | solution.py:156
  197.8 0.0 copy-done.3
  197.8 2.0 mix.1
  (1 shorter events, 0.0 us)
Async XLA Ops:
  0.0 0.7 copy-start.6
  0.0 0.9 copy-start.5
  0.0 1.1 copy-start.4
  1.1 108.1 %copy-start.1 = (bf16[1,2048,512]{2,1,0:T(8,128)(2,1)S(1)}, bf16[1,2048,512]{2,1,0:T(8,128)(2,1)}, u32[]{:S(2)}) copy-start(bf16[1,2048,512]{2,1,0:T(8,128)(2,1)} %param.12) | copy-start | bytes 6291460
  1.1 108.1 %copy-start.2 = (bf16[1,512,2048]{2,1,0:T(8,128)(2,1)S(1)}, bf16[1,512,2048]{2,1,0:T(8,128)(2,1)}, u32[]{:S(2)}) copy-start(bf16[1,512,2048]{2,1,0:T(8,128)(2,1)} %param.13) | copy-start | bytes 6291460
  2.3 106.9 %copy-start = (bf16[1,2048,512]{2,1,0:T(8,128)(2,1)S(1)}, bf16[1,2048,512]{2,1,0:T(8,128)(2,1)}, u32[]{:S(2)}) copy-start(bf16[1,2048,512]{2,1,0:T(8,128)(2,1)} %param.11) | copy-start | bytes 6291460
  112.7 85.1 %copy-start.3 = (f32[128,2]{0,1:T(2,128)S(1)}, f32[128,2]{0,1:T(2,128)}, u32[]{:S(2)}) copy-start(f32[128,2]{0,1:T(2,128)} %param.10) | copy-start | bytes 3076

commit v6 on v5

--- a/solution.py
+++ b/solution.py
@@ -52,7 +52,7 @@
             rows_ref[g + tiles : g + 2 * tiles, c * LANES : (c + 1) * LANES] = part[:, LANES:]
 
 
-def table_kernel(capacity, ids_ref, table_ref, *pick_refs):
+def table_kernel(capacity, ids_ref, table_ref, picks_ref):
     n, tok_rows = table_ref.shape
     row = lax.broadcasted_iota(jnp.int32, (n, tok_rows), 0)
     expert = lax.div(row, capacity)
@@ -66,8 +66,8 @@
     rank = jnp.dot(named.astype(jnp.bfloat16), earlier, preferred_element_type=jnp.float32)
     in_slot = rank == lax.rem(row, capacity).astype(jnp.float32)
     table_ref[...] = (named & in_slot).astype(jnp.bfloat16)
-    for pick, pick_ref in zip(picks, pick_refs):
-        pick_ref[...] = (pick & in_slot).astype(jnp.bfloat16)
+    for k, pick in enumerate(picks):
+        picks_ref[:, k * tok_rows : (k + 1) * tok_rows] = (pick & in_slot).astype(jnp.bfloat16)
 
 
 def dispatch_kernel(tokens_ref, gain_ref, table_ref, swap_ref, out_ref, rows_ref):
@@ -98,8 +98,7 @@
     spread_rows(table, rows_ref, out_ref)
 
 
-def mix_kernel(swap_ref, in_ref, weights_ref, *refs):
-    *pick_refs, out_hbm, rows_ref, mixed_ref, sems = refs
+def mix_kernel(swap_ref, in_ref, weights_ref, picks_ref, out_hbm, rows_ref, mixed_ref, sems):
     width = mixed_ref.shape[1]
     gather_rows(swap_ref[...], in_ref, rows_ref)
     top_count, tok_rows = weights_ref.shape
@@ -109,15 +108,15 @@
     copies = []
     for i in range(sems.shape[0]):
         columns = slice(i * step, (i + 1) * step)
+        picked = lax.dot_general(
+            picks_ref[...],
+            rows_ref[:, columns],
+            (((0,), (0,)), ((), ())),
+            preferred_element_type=jnp.float32,
+        )
         total = None
-        for k, pick_ref in enumerate(pick_refs):
-            picked = lax.dot_general(
-                pick_ref[...],
-                rows_ref[:, columns],
-                (((0,), (0,)), ((), ())),
-                preferred_element_type=jnp.float32,
-            )
-            term = picked * weights[:, k : k + 1]
+        for k in range(top_count):
+            term = picked[k * tok_rows : (k + 1) * tok_rows] * weights[:, k : k + 1]
             total = term if total is None else total + term
         mixed_ref[:, columns] = total.astype(mixed_ref.dtype)
         copy = pltpu.make_async_copy(mixed_ref.at[:, columns], out_hbm.at[:, columns], sems.at[i])
@@ -165,9 +164,12 @@
         AHEAD,
         4,
     )
-    table, *picks = call(
+    table, picks = call(
         lambda *refs: table_kernel(capacity, *refs),
-        [jax.ShapeDtypeStruct((n, tok_rows), jnp.bfloat16)] * (1 + top_count),
+        [
+            jax.ShapeDtypeStruct((n, tok_rows), jnp.bfloat16),
+            jax.ShapeDtypeStruct((n, top_count * tok_rows), jnp.bfloat16),
+        ],
         [route_ids.T],
         [],
         "table",
@@ -200,11 +202,11 @@
     return call(
         mix_kernel,
         jax.ShapeDtypeStruct(tokens.shape, tokens.dtype),
-        [swap, returned, route_weights.T, *picks],
+        [swap, returned, route_weights.T, picks],
         [
             rows_scratch,
             pltpu.VMEM(tokens.shape, tokens.dtype),
-            pltpu.SemaphoreType.DMA((4,)),
+            pltpu.SemaphoreType.DMA((2,)),
         ],
         "mix",
         2 * top_count * n * tok_rows * width,

time: 200 us -> 200 us (level)
  no operation moved by 1% of the time
where the time goes in v6:
time: 200 us
  blocking collectives  192 us (96%)
  Pallas kernels  7.01 us (4%)
    all_to_all x2, blocking collectives, exchange(): lax.all_to_all(blocks, AXES, split_axis=0, concat_axis=0, tiled=True)  192 us
    pallas_call x5, Pallas kernels, call(): pl.pallas_call(kernel, out_shape=out_shape, in_specs=[OUTSIDE if i in out...  7.01 us

profile of v6, /device:TPU:33, one launch (start us, length us, event | category | flops | bytes accessed | tf_op | source)
XLA Modules:
  0.0 199.8 jit_solution(5907043289285399398)
XLA Ops:
  0.0 0.0 copy-start.6
  0.0 0.0 copy-start.5
  0.0 0.0 copy-start.4
  0.1 0.6 copy-done.6
  0.7 0.2 table.1
  0.9 0.0 copy-done.5
  0.9 0.2 copy-done.4
  1.1 0.0 copy-start.1
  1.1 0.0 copy-start.2
  1.1 1.2 dispatch.1
  2.3 0.0 copy-start
  2.3 106.9 %all_to_all.10 = bf16[128,48,128]{2,1,0:T(8,128)(2,1)S(1)} all-to-all(bf16[128,48,128]{2,1,0:T(8,128)(2,1)S(1)} %bitcast.16), channel_id=1, replica_groups=mesh['grp'=2,'ep'=32,'tp'=4] {'ep','tp'}, dimensions={0} | all-to-all | bytes 3145728 | tf_op jit(solution)/shard_map/all_to_all | solution.py:155
  109.2 0.0 copy-done.1
  109.2 0.0 copy-done.2
  109.2 0.0 copy-done
  109.2 3.5 %products.1 = bf16[6144,128]{1,0:T(8,128)(2,1)S(1)} custom-call(bf16[256,256]{1,0:T(8,128)(2,1)S(1)} %swap.1.swap_ref, bf16[6144,128]{1,0:T(8,128)(2,1)S(1)} %bitcast.11, bf16[2048,512]{1,0:T(8,128)(2,1)S(1)} %bitcast.13, bf16[2048,512]{1,0:T(8,128)(2,1)S(1)} %bitcast.14, bf16[512,2048]{1,0:T(8,128)(2,1)S(1)} %bitcast.15), custom_call_target="tpu_custom_call" | custom-call | flops 2415919104 | bytes 4194304 | tf_op jit(solution)/shard_map/products/pallas_call | solution.py:142
  112.7 0.0 copy-start.3
  112.8 85.1 %all_to_all.11 = bf16[128,48,128]{2,1,0:T(8,128)(2,1)S(1)} all-to-all(bf16[128,48,128]{2,1,0:T(8,128)(2,1)S(1)} %bitcast.12), channel_id=1, replica_groups=mesh['grp'=2,'ep'=32,'tp'=4] {'ep','tp'}, dimensions={0} | all-to-all | bytes 3145728 | tf_op jit(solution)/shard_map/all_to_all | solution.py:155
  197.8 0.0 copy-done.3
  197.8 2.0 mix.1
  (1 shorter events, 0.0 us)
Async XLA Ops:
  0.0 0.7 copy-start.6
  0.0 0.9 copy-start.5
  0.0 1.1 copy-start.4
  1.1 108.1 %copy-start.1 = (bf16[1,2048,512]{2,1,0:T(8,128)(2,1)S(1)}, bf16[1,2048,512]{2,1,0:T(8,128)(2,1)}, u32[]{:S(2)}) copy-start(bf16[1,2048,512]{2,1,0:T(8,128)(2,1)} %param.12) | copy-start | bytes 6291460
  1.1 108.1 %copy-start.2 = (bf16[1,512,2048]{2,1,0:T(8,128)(2,1)S(1)}, bf16[1,512,2048]{2,1,0:T(8,128)(2,1)}, u32[]{:S(2)}) copy-start(bf16[1,512,2048]{2,1,0:T(8,128)(2,1)} %param.13) | copy-start | bytes 6291460
  2.3 106.9 %copy-start = (bf16[1,2048,512]{2,1,0:T(8,128)(2,1)S(1)}, bf16[1,2048,512]{2,1,0:T(8,128)(2,1)}, u32[]{:S(2)}) copy-start(bf16[1,2048,512]{2,1,0:T(8,128)(2,1)} %param.11) | copy-start | bytes 6291460
  112.7 85.1 %copy-start.3 = (f32[128,2]{0,1:T(2,128)S(1)}, f32[128,2]{0,1:T(2,128)}, u32[]{:S(2)}) copy-start(f32[128,2]{0,1:T(2,128)} %param.10) | copy-start | bytes 3076
